TPU v7x, 128 devices: a whole 4x4x4 slice. The times are simulated.
128 devices in a mesh: sp: 64 (over z, y, x), tp: 2 (over core).
Axes of the slice: x: 4, y: 4, z: 4, core: 2. Of those that a mesh axis runs over, the one named last changes fastest.
Arguments:
- pool_input: bfloat16 [16384, 1024], P('sp', 'tp'), may hold values from -6 to 6
- residual: bfloat16 [16384, 2048], P(('sp', 'tp')), may hold values from -6 to 6
- pool_weight: bfloat16 [4, 256, 256], replicated, may hold values from -0.375 to 0.375
- pool_gain: float32 [1024], replicated, may hold values from 0.1 to 1.9
- out_weight: bfloat16 [1024, 2048], replicated, may hold values from -0.1875 to 0.1875
- norm_gain: float32 [2048], replicated, may hold values from 0.1 to 1.9
- routes: int32 [16384, 4], P(('sp', 'tp')), may hold values from 0 to 63, all different within a row; in each aligned block of 128 rows (0 to 127, 128 to 255, ...) at most 16 rows name the same one
- route_scores: float32 [16384, 4], P(('sp', 'tp')), may hold values from -1 to 1
- gate_weight: bfloat16 [64, 2048, 2048], P('sp', None, 'tp'), may hold values from -0.375 to 0.375
- up_weight: bfloat16 [64, 2048, 2048], P('sp', None, 'tp'), may hold values from -0.375 to 0.375
- down_weight: bfloat16 [64, 2048, 2048], P('sp', 'tp'), may hold values from -0.0234375 to 0.0234375
Outputs:
- layer_out: bfloat16 [16384, 2048], P(('sp', 'tp'))
Inputs may be any that keep to these rules, and one draw needn't show every extreme that they name: `routes`: each row names 4 different experts; among the rows of one device no expert is named more than 16 times, a bound that some block reaches.
All inputs are finite; a program needn't handle non-finite values.
Results may differ from a plain program's by a relative error of at most 0.012.
Values may be sent and summed in bfloat16 or wider, within the bound.
No kernel may reach another device: no remote copies, remote signals or barrier semaphores. Data moves between devices by JAX's collectives and lax.ppermute only.
A program may use at most 128 MiB of HBM per device.

v0:
```python
import jax
import jax.numpy as jnp
from jax import lax
from jax.sharding import PartitionSpec as P


def from_behind(block, axis, distance):
    devices = range(lax.axis_size(axis))
    route = [(i - distance, i) for i in devices if i - distance in devices]
    return lax.ppermute(block, axis, route)


def in_blocks(x, dim, devices):
    before, after = (x.shape[:dim], x.shape[dim + 1 :])
    return jnp.moveaxis(x.reshape(*before, devices, -1, *after), dim, 0)


def sent_and_summed(x, axis, dim):
    devices = lax.axis_size(axis)
    parts = lax.all_to_all(in_blocks(x, dim, devices), axis, 0, 0, tiled=True)
    return jnp.sum(parts.astype(jnp.float32), axis=0)


def expert_half(rows, gate_local, up_local, down_local):
    gate_pre = jnp.dot(rows, gate_local, preferred_element_type=jnp.float32)
    up_pre = jnp.dot(rows, up_local, preferred_element_type=jnp.float32)
    clipped_gate = jnp.minimum(gate_pre, 7.0)
    clipped_up = jnp.clip(up_pre, -7.0, 7.0)
    activated = ((clipped_up + 1.0) * (clipped_gate * jax.nn.sigmoid(1.702 * clipped_gate))).astype(
        jnp.bfloat16
    )
    return jnp.dot(activated, down_local, preferred_element_type=jnp.float32).astype(jnp.bfloat16)


def shards(
    pool_input,
    residual,
    pool_weight,
    pool_gain,
    out_weight,
    norm_gain,
    routes,
    route_scores,
    gate_weight,
    up_weight,
    down_weight,
):
    tokens_here, width_here = pool_input.shape
    cores = lax.axis_size("tp")
    groups_here = pool_weight.shape[0] // cores
    group_dim = pool_weight.shape[1]
    core_index = lax.axis_index("tp")
    first_group = core_index * groups_here
    previous = from_behind(pool_input[tokens_here - 16 :], "sp", 1)
    extended = jnp.concatenate([previous, pool_input], axis=0).astype(jnp.float32)
    channel_group = first_group + jnp.arange(width_here) // group_dim
    windows = jnp.left_shift(jnp.int32(2), channel_group).astype(jnp.float32)
    totals = jnp.zeros((tokens_here, width_here), jnp.float32)
    for offset in range(16):
        keeper = (windows > offset).astype(jnp.float32)
        totals = totals + extended[16 - offset : 16 - offset + tokens_here] * keeper[None, :]
    positions = (lax.axis_index("sp") * tokens_here + jnp.arange(tokens_here)).astype(jnp.float32)
    counts = jnp.minimum(positions[:, None] + 1.0, windows[None, :])
    pooled = (totals / counts - pool_input.astype(jnp.float32)).astype(jnp.bfloat16)
    local_weight = lax.dynamic_slice_in_dim(pool_weight, first_group, groups_here, 0)
    local_gain = lax.dynamic_slice_in_dim(pool_gain, first_group * group_dim, width_here, 0)
    grouped = jnp.einsum(
        "tgc,gce->tge",
        pooled.reshape(tokens_here, groups_here, group_dim),
        local_weight,
        preferred_element_type=jnp.float32,
    )
    mixer_out = (grouped.reshape(tokens_here, width_here) * local_gain[None, :]).astype(
        jnp.bfloat16
    )
    token_rows = lax.all_to_all(mixer_out, "tp", split_axis=0, concat_axis=1, tiled=True)
    projected = jnp.dot(token_rows, out_weight, preferred_element_type=jnp.float32)
    middle = (residual.astype(jnp.float32) + projected).astype(jnp.bfloat16)
    middle_wide = middle.astype(jnp.float32)
    normed = (
        middle_wide
        * lax.rsqrt(jnp.mean(middle_wide * middle_wide, axis=1, keepdims=True) + 1e-05)
        * norm_gain[None, :]
    ).astype(jnp.bfloat16)
    weights = jax.nn.softmax(route_scores, axis=-1)
    row_count, top_count = routes.shape
    model_width = normed.shape[1]
    experts_total = gate_weight.shape[0] * lax.axis_size("sp")
    capacity = row_count * top_count * cores // experts_total
    slots_total = experts_total * capacity
    flat_expert = routes.reshape(-1)
    onehot = (flat_expert[:, None] == jnp.arange(experts_total)[None, :]).astype(jnp.int32)
    ranks = jnp.sum((jnp.cumsum(onehot, axis=0) - 1) * onehot, axis=1)
    slot_ids = flat_expert * capacity + ranks
    picker = jnp.any(
        (jnp.arange(slots_total)[:, None] == slot_ids[None, :]).reshape(
            slots_total, row_count, top_count
        ),
        axis=2,
    ).astype(jnp.bfloat16)
    outgoing = (
        jnp.dot(picker, normed, preferred_element_type=jnp.float32)
        .astype(jnp.bfloat16)
        .reshape(experts_total, capacity, model_width)
    )
    gate_local = gate_weight[0]
    up_local = up_weight[0]
    down_local = down_weight[0]
    paired = lax.all_gather(
        lax.all_to_all(outgoing, "sp", split_axis=0, concat_axis=0, tiled=True),
        "tp",
        axis=0,
        tiled=True,
    )
    partial_value = expert_half(
        paired.reshape(-1, model_width), gate_local, up_local, down_local
    ).reshape(paired.shape)
    summed = sent_and_summed(partial_value, "tp", 0).astype(jnp.bfloat16)
    expert_out = lax.all_to_all(summed, "sp", split_axis=0, concat_axis=0, tiled=True)
    expert_flat = expert_out.reshape(slots_total, model_width)
    route_rows = (
        expert_flat[slot_ids].astype(jnp.float32).reshape(row_count, top_count, model_width)
    )
    mixture = jnp.sum(route_rows * weights[:, :, None], axis=1)
    return (middle_wide + mixture).astype(jnp.bfloat16)


def solution(mesh):
    return jax.shard_map(
        shards,
        mesh=mesh,
        in_specs=(
            P("sp", "tp"),
            P(("sp", "tp"), None),
            P(),
            P(),
            P(),
            P(),
            P(("sp", "tp"), None),
            P(("sp", "tp"), None),
            P("sp", None, "tp"),
            P("sp", None, "tp"),
            P("sp", "tp", None),
        ),
        out_specs=P(("sp", "tp"), None),
        check_vma=False,
    )
```

profile of v0, /device:TPU:1, one launch (start us, length us, event | category | flops | bytes accessed | tf_op | source)
XLA Modules:
  0.0 270.1 jit_solution(11678458812910446133)
XLA Ops:
  6.5 0.0 copy-start
  6.5 0.0 all-gather.2.cloned.1.call-start
  6.5 0.8 slice.57
  7.3 3.9 %collective-permute-start = (bf16[16,512]{1,0:T(8,128)(2,1)S(1)}, bf16[16,512]{1,0:T(8,128)(2,1)S(1)}, u32[]{:S(2)}, u32[]{:S(2)}) collective-permute-start(bf16[16,512]{1,0:T(8,128)(2,1)S(1)} %slice.57), channel_id=1, source_target_pairs={{0,2},{2,4},{4,6},{6,8},{8,10},{10,12},{12,14},{14,16},{16,18},{18... | collective-permute-start | bytes 49160 | tf_op jit(solution)/shard_map/ppermute | solution.py:10
  11.4 0.8 copy.35
  12.2 0.1 eq.44
  12.3 0.1 eq.40
  12.4 1.2 reduce-window.6
  13.6 0.2 slice_reduce_fusion
  13.9 0.1 fusion.37
  14.0 0.1 reduce_sum.53
  14.2 0.1 copy.39
  14.2 0.4 fusion.11
  14.6 0.8 dynamic_slice.7
  15.4 0.0 collective-permute-done
  15.4 1.0 maximum_convert_fusion
  16.4 0.0 copy-start.2
  16.4 2.0 fusion.32
  18.4 0.0 copy-done
  18.4 0.3 convolution_bitcast_fusion
  18.7 0.0 copy-start.4
  18.7 0.3 reshape.194
  19.0 0.1 fusion.29
  19.1 4.5 %all_to_all.31 = bf16[2,128,512]{1,2,0:T(8,128)(2,1)S(1)} all-to-all(bf16[2,128,512]{1,2,0:T(8,128)(2,1)S(1)} %fusion.29), channel_id=1, replica_groups=mesh['sp'=64,'tp'=2] {'tp'}, dimensions={0} | all-to-all | bytes 524288 | tf_op jit(solution)/shard_map/all_to_all | solution.py:76
  23.7 0.0 copy-done.2
  23.7 3.0 %multiply_reduce_fusion.1 = (f32[128]{0:T(128)S(1)}, f32[128,2048]{1,0:T(8,128)S(1)}) fusion(bf16[128,1024]{0,1:T(8,128)(2,1)S(1)} %bitcast.49, bf16[1024,2048]{1,0:T(8,128)(2,1)} %param.15, bf16[128,2048]{1,0:T(8,128)(2,1)S(1)} %copy-done.2), kind=kOutput, calls=%fused_computation.21 | convolution fusion | flops 538443648 | bytes 6029824 | tf_op jit(solution)/shard_map/dot_general | solution.py:77
  26.7 0.0 copy-done.4
  26.7 1.3 convolution_convert_fusion.1
  28.0 62.3 %all_to_all.32 = bf16[64,16,2048]{2,1,0:T(8,128)(2,1)} all-to-all(bf16[64,16,2048]{2,1,0:T(8,128)(2,1)S(1)} %bitcast.47), channel_id=1, replica_groups=mesh['sp'=64,'tp'=2] {'sp'}, dimensions={0} | all-to-all | bytes 8388608 | tf_op jit(solution)/shard_map/all_to_all | solution.py:110
  90.4 0.0 all-gather.2.cloned.1.call-update
  90.4 21.0 %all-gather.2.cloned.1.call-done = bf16[128,16,2048]{2,1,0:T(8,128)(2,1)} async-done(((bf16[64,16,2048]{2,1,0:T(8,128)(2,1)}), bf16[128,16,2048]{2,1,0:T(8,128)(2,1)}) %all-gather.2.cloned.1.call-update) | async-done | bytes 8388624 | tf_op jit(solution)/shard_map/all_gather | solution.py:109
  111.4 14.4 %fusion.1 = f32[2048,1024]{1,0:T(8,128)} fusion(bf16[2048,2048]{1,0:T(8,128)(2,1)} %bitcast.53, bf16[1,2048,1024]{2,1,0:T(8,128)(2,1)} %param.19), kind=kOutput, calls=%fused_computation.4 | convolution fusion | flops 8589934592 | bytes 20971520 | tf_op jit(solution)/shard_map/dot_general | solution.py:25
  125.9 26.9 %convolution_convert_fusion = bf16[2048,2048]{1,0:T(8,128)(2,1)} fusion(f32[2048,1024]{1,0:T(8,128)} %fusion.1, bf16[2048,2048]{1,0:T(8,128)(2,1)} %bitcast.54, bf16[1,1024,2048]{2,1,0:T(8,128)(2,1)} %param.21, bf16[1,2048,1024]{2,1,0:T(8,128)(2,1)} %param.20), kind=kOutput, calls=%fused_computation.2 | convolution fusion | flops 17205035008 | bytes 33554432 | tf_op jit(solution)/shard_map/dot_general | solution.py:32
  152.8 18.4 %all_to_all.33 = bf16[2,64,16,2048]{3,2,1,0:T(8,128)(2,1)} all-to-all(bf16[2,64,16,2048]{3,2,1,0:T(8,128)(2,1)} %bitcast.48), channel_id=1, replica_groups=mesh['sp'=64,'tp'=2] {'tp'}, dimensions={0} | all-to-all | bytes 16777216 | tf_op jit(solution)/shard_map/all_to_all | solution.py:20
  171.2 8.9 %reduce_sum.55 = bf16[64,16,2048]{2,1,0:T(8,128)(2,1)} reduce(bf16[2,64,16,2048]{3,2,1,0:T(8,128)(2,1)} %all_to_all.33, bf16[]{:T(256)} %constant.130.clone.1), dimensions={0}, to_apply=%region_5.6 | reduce | flops 2097152 | bytes 12582914 | tf_op jit(solution)/shard_map/reduce_sum | solution.py:21
  180.1 0.0 copy-start.3
  180.1 10.5 %all-to-all-start.3 = ((bf16[64,16,2048]{2,1,0:T(8,128)(2,1)}), bf16[64,16,2048]{2,1,0:T(8,128)(2,1)}, u32[]{:S(2)}, u32[]{:S(2)}) async-start(bf16[64,16,2048]{2,1,0:T(8,128)(2,1)} %reduce_sum.55), calls=%async_computation.3 | async-start | bytes 8388608 | tf_op jit(solution)/shard_map/all_to_all | solution.py:119
  190.6 0.1 mul.257
  190.7 0.0 copy-done.3
  190.8 0.1 copy.40
  190.9 53.1 %all-to-all-done.3 = bf16[64,16,2048]{2,1,0:T(8,128)(2,1)} async-done(((bf16[64,16,2048]{2,1,0:T(8,128)(2,1)}), bf16[64,16,2048]{2,1,0:T(8,128)(2,1)}, u32[]{:S(2)}, u32[]{:S(2)}) %all-to-all-start.3) | async-done | bytes 4194336 | tf_op jit(solution)/shard_map/all_to_all | solution.py:119
  244.0 8.0 %gather_fusion = bf16[512,2048]{1,0:T(8,128)(2,1)} fusion(bf16[1024,2048]{1,0:T(8,128)(2,1)} %bitcast.10, s32[1024]{0:T(1024)S(1)} %pad_clamp_fusion), kind=kCustom, calls=%fused_computation | custom fusion | bytes 4196352 | tf_op jit(solution)/shard_map/gather | solution.py:122
  252.0 0.0 copy-start.1
  252.0 4.8 %reshape.199 = f32[128,4,2048]{2,1,0:T(4,128)} reshape(bf16[512,2048]{1,0:T(8,128)(2,1)} %gather_fusion) | data formatting | bytes 6291456 | tf_op jit(solution)/shard_map/convert_element_type | solution.py:122
  256.8 5.4 %multiply_reduce_fusion = f32[128,2048]{1,0:T(8,128)S(1)} fusion(f32[128,4,2048]{2,1,0:T(4,128)} %reshape.199, f32[128,4]{1,0:T(8,128)S(1)} %copy.40), kind=kLoop, calls=%fused_computation.7 | loop fusion | flops 1835008 | bytes 5244928 | tf_op jit(solution)/shard_map/reduce_sum | solution.py:124
  262.3 0.9 add_convert_fusion
  263.2 0.0 copy-done.1
  (20 shorter events, 0.2 us)
Async XLA Ops:
  6.5 11.9 %copy-start = (bf16[4,256,256]{2,1,0:T(8,128)(2,1)S(1)}, bf16[4,256,256]{2,1,0:T(8,128)(2,1)}, u32[]{:S(2)}) copy-start(bf16[4,256,256]{2,1,0:T(8,128)(2,1)} %param.13) | copy-start | bytes 1572868
  6.5 104.9 %all-gather.2.cloned.1.call-start = ((), (), s32[]{:S(2)}) async-start(), calls=%async_computation.4 | async-start | bytes 12582912 | tf_op jit(solution)/shard_map/all_gather | solution.py:109
  7.3 8.1 %collective-permute-start = (bf16[16,512]{1,0:T(8,128)(2,1)S(1)}, bf16[16,512]{1,0:T(8,128)(2,1)S(1)}, u32[]{:S(2)}, u32[]{:S(2)}) collective-permute-start(bf16[16,512]{1,0:T(8,128)(2,1)S(1)} %slice.57), channel_id=1, source_target_pairs={{0,2},{2,4},{4,6},{6,8},{8,10},{10,12},{12,14},{14,16},{16,18},{18... | collective-permute-start | bytes 49160 | tf_op jit(solution)/shard_map/ppermute | solution.py:10
  16.4 7.3 %copy-start.2 = (bf16[128,2048]{1,0:T(8,128)(2,1)S(1)}, bf16[128,2048]{1,0:T(8,128)(2,1)}, u32[]{:S(2)}) copy-start(bf16[128,2048]{1,0:T(8,128)(2,1)} %param.12) | copy-start | bytes 1572868
  18.7 8.0 %copy-start.4 = (f32[2048]{0:T(1024)S(1)}, f32[2048]{0:T(1024)}, u32[]{:S(2)}) copy-start(f32[2048]{0:T(1024)} %param.16) | copy-start | bytes 24580
  180.1 10.6 %copy-start.3 = (f32[128,4]{0,1:T(4,128)S(1)}, f32[128,4]{0,1:T(4,128)}, u32[]{:S(2)}) copy-start(f32[128,4]{0,1:T(4,128)} %param.18) | copy-start | bytes 6148
  180.1 63.9 %all-to-all-start.3 = ((bf16[64,16,2048]{2,1,0:T(8,128)(2,1)}), bf16[64,16,2048]{2,1,0:T(8,128)(2,1)}, u32[]{:S(2)}, u32[]{:S(2)}) async-start(bf16[64,16,2048]{2,1,0:T(8,128)(2,1)} %reduce_sum.55), calls=%async_computation.3 | async-start | bytes 8388608 | tf_op jit(solution)/shard_map/all_to_all | solution.py:119
  252.0 11.2 %copy-start.1 = (bf16[4,256,256]{2,1,0:T(8,128)(2,1)S(1)}, bf16[4,256,256]{2,1,0:T(8,128)(2,1)}, u32[]{:S(2)}) copy-start(bf16[4,256,256]{2,1,0:T(8,128)(2,1)} %param.13) | copy-start | bytes 1572868
Sparse Core Ops, SparseCore 0:
  90.5 20.8 all-gather.1
where the time goes:
time: 271 us; the launch traced here: 270 us
  blocking collectives  85.3 us (31%)
  waiting for transfers between devices  74.2 us (27%)
  matrix products  45.9 us (17%)
  other arithmetic  20.3 us (7%)
  local copies, waits for them, and re-layouts  16.3 us (6%)
  starting transfers between devices  14.4 us (5%)
  between operations  13.6 us (5%)
    all_to_all x1, blocking collectives, shards(): lax.all_to_all(outgoing, 'sp', split_axis=0, concat_axis=0, tiled=True)  62.3 us
    all_to_all x1, waiting for transfers between devices, shards(): lax.all_to_all(summed, 'sp', split_axis=0, concat_axis=0, tiled=True)  53.1 us
    dot_general x1, matrix products, expert_half(): jnp.dot(activated, down_local, preferred_element_type=jnp.float32)  26.9 us
    all_gather x1, waiting for transfers between devices, shards(): lax.all_gather(lax.all_to_all(outgoing, 'sp', split_axis=0, concat_axis=0...  21 us
    all_to_all x1, blocking collectives, sent_and_summed(): parts = lax.all_to_all(in_blocks(x, dim, devices), axis, 0, 0, tiled=True)  18.4 us
    dot_general x1, matrix products, expert_half(): gate_pre = jnp.dot(rows, gate_local, preferred_element_type=jnp.float32)  14.4 us
    all_to_all x1, starting transfers between devices, shards(): lax.all_to_all(summed, 'sp', split_axis=0, concat_axis=0, tiled=True)  10.5 us
    reduce_sum x1, other arithmetic, sent_and_summed(): return jnp.sum(parts.astype(jnp.float32), axis=0)  8.89 us
  transfers between devices with their start and end apart: 3, of which 2 were waited for; matrix products, arithmetic and copies ran while one was open for 2% of the time, Pallas kernels for 0%

commit v1 on v0

--- a/solution.py
+++ b/solution.py
@@ -10,26 +10,14 @@
     return lax.ppermute(block, axis, route)
 
 
-def in_blocks(x, dim, devices):
-    before, after = (x.shape[:dim], x.shape[dim + 1 :])
-    return jnp.moveaxis(x.reshape(*before, devices, -1, *after), dim, 0)
-
-
-def sent_and_summed(x, axis, dim):
-    devices = lax.axis_size(axis)
-    parts = lax.all_to_all(in_blocks(x, dim, devices), axis, 0, 0, tiled=True)
-    return jnp.sum(parts.astype(jnp.float32), axis=0)
-
-
-def expert_half(rows, gate_local, up_local, down_local):
-    gate_pre = jnp.dot(rows, gate_local, preferred_element_type=jnp.float32)
-    up_pre = jnp.dot(rows, up_local, preferred_element_type=jnp.float32)
+def hidden_half(rows, gate_half, up_half):
+    gate_pre = jnp.dot(rows, gate_half, preferred_element_type=jnp.float32)
+    up_pre = jnp.dot(rows, up_half, preferred_element_type=jnp.float32)
     clipped_gate = jnp.minimum(gate_pre, 7.0)
     clipped_up = jnp.clip(up_pre, -7.0, 7.0)
-    activated = ((clipped_up + 1.0) * (clipped_gate * jax.nn.sigmoid(1.702 * clipped_gate))).astype(
+    return ((clipped_up + 1.0) * (clipped_gate * jax.nn.sigmoid(1.702 * clipped_gate))).astype(
         jnp.bfloat16
     )
-    return jnp.dot(activated, down_local, preferred_element_type=jnp.float32).astype(jnp.bfloat16)
 
 
 def shards(
@@ -45,6 +33,10 @@
     up_weight,
     down_weight,
 ):
+    swap = [(0, 1), (1, 0)]
+    other_gate = lax.ppermute(gate_weight[0], "tp", swap)
+    other_up = lax.ppermute(up_weight[0], "tp", swap)
+    other_down = lax.ppermute(down_weight[0], "tp", swap)
     tokens_here, width_here = pool_input.shape
     cores = lax.axis_size("tp")
     groups_here = pool_weight.shape[0] // cores
@@ -103,25 +95,30 @@
         .astype(jnp.bfloat16)
         .reshape(experts_total, capacity, model_width)
     )
-    gate_local = gate_weight[0]
-    up_local = up_weight[0]
-    down_local = down_weight[0]
-    paired = lax.all_gather(
-        lax.all_to_all(outgoing, "sp", split_axis=0, concat_axis=0, tiled=True),
-        "tp",
-        axis=0,
-        tiled=True,
+    received = lax.all_to_all(outgoing, "sp", split_axis=0, concat_axis=0, tiled=True)
+    rows = received.reshape(-1, model_width)
+    own = hidden_half(rows, gate_weight[0], up_weight[0])
+    other = hidden_half(rows, other_gate, other_up)
+    expert_rows = (
+        jnp.dot(own, down_weight[0], preferred_element_type=jnp.float32)
+        + jnp.dot(other, other_down, preferred_element_type=jnp.float32)
+    ).astype(jnp.bfloat16)
+    returned = lax.all_to_all(
+        expert_rows.reshape(received.shape), "sp", split_axis=0, concat_axis=0, tiled=True
+    ).reshape(slots_total, model_width)
+    spread = jnp.sum(
+        jnp.where(
+            (jnp.arange(slots_total)[None, None, :] == slot_ids.reshape(row_count, top_count)[:, :, None]),
+            weights[:, :, None],
+            0.0,
+        ),
+        axis=1,
     )
-    partial_value = expert_half(
-        paired.reshape(-1, model_width), gate_local, up_local, down_local
-    ).reshape(paired.shape)
-    summed = sent_and_summed(partial_value, "tp", 0).astype(jnp.bfloat16)
-    expert_out = lax.all_to_all(summed, "sp", split_axis=0, concat_axis=0, tiled=True)
-    expert_flat = expert_out.reshape(slots_total, model_width)
-    route_rows = (
-        expert_flat[slot_ids].astype(jnp.float32).reshape(row_count, top_count, model_width)
+    high = spread.astype(jnp.bfloat16)
+    low = (spread - high.astype(jnp.float32)).astype(jnp.bfloat16)
+    mixture = jnp.dot(high, returned, preferred_element_type=jnp.float32) + jnp.dot(
+        low, returned, preferred_element_type=jnp.float32
     )
-    mixture = jnp.sum(route_rows * weights[:, :, None], axis=1)
     return (middle_wide + mixture).astype(jnp.bfloat16)
 
 

time: 271 us -> 214 us (0.79)
  blocking collectives: 85.3 us -> 4.53 us
  waiting for transfers between devices: 74.2 us -> 104 us
  matrix products: 45.9 us -> 67.7 us
  other arithmetic: 20.3 us -> 6.01 us
  between operations: 13.6 us -> 0.22 us
  local copies, waits for them, and re-layouts: 16.3 us -> 3.24 us
  starting transfers between devices: 14.4 us -> 26.3 us
    all_to_all x2 -> x0, blocking collectives: 80.8 us -> none  [the longest x1 62.3 us: shards(): lax.all_to_all(outgoing, 'sp', split_axis=0, concat_axis=0, tiled=True)]
    all_to_all x1 -> x2, waiting for transfers between devices: 53.1 us -> 104 us  [the longest x1 52.2 us: shards(): lax.all_to_all(outgoing, 'sp', split_axis=0, concat_axis=0, tiled=True)]
    all_gather x1 -> x0, waiting for transfers between devices: 21 us -> none  [shards(): lax.all_gather(lax.all_to_all(outgoing, 'sp', split_axis=0, concat_axis=0...]
    dot_general x2 -> x6, matrix products: 41.3 us -> 61.2 us  [the longest x2 19.9 us: hidden_half(): up_pre = jnp.dot(rows, up_half, preferred_element_type=jnp.float32)]
    reduce_sum x2 -> x1, other arithmetic: 14.3 us -> 0.3 us  [shards(): jnp.sum(jnp.where(jnp.arange(slots_total)[None, None, :] == slot_ids.resh...]
    all_to_all x1 -> x2, starting transfers between devices: 10.5 us -> 21.1 us  [the longest x1 11.1 us: shards(): lax.all_to_all(outgoing, 'sp', split_axis=0, concat_axis=0, tiled=True)]
    gather x1 -> x0, local copies, waits for them, and re-layouts: 8 us -> none  [shards(): expert_flat[slot_ids].astype(jnp.float32)]
    convert_element_type x1 -> x0, local copies, waits for them, and re-layouts: 4.81 us -> none  [shards(): expert_flat[slot_ids].astype(jnp.float32)]
  transfers between devices with their start and end apart: 3 -> 6, of which waited for: 2 -> 2; matrix products, arithmetic and copies ran while one was open for 2% -> 20% of each run, Pallas kernels for 0% -> 0%
where the time goes in v1:
time: 214 us; the launch traced here: 212 us
  waiting for transfers between devices  104 us (49%)
  matrix products  67.7 us (32%)
  starting transfers between devices  26.3 us (12%)
  other arithmetic  6.01 us (3%)
  blocking collectives  4.53 us (2%)
  local copies, waits for them, and re-layouts  3.24 us (2%)
    all_to_all x1, waiting for transfers between devices, shards(): lax.all_to_all(outgoing, 'sp', split_axis=0, concat_axis=0, tiled=True)  52.2 us
    all_to_all x1, waiting for transfers between devices, shards(): lax.all_to_all(expert_rows.reshape(received.shape), 'sp', split_axis=0, c...  52.1 us
    dot_general x2, matrix products, hidden_half(): up_pre = jnp.dot(rows, up_half, preferred_element_type=jnp.float32)  19.9 us
    dot_general x1, matrix products, shards(): jnp.dot(other, other_down, preferred_element_type=jnp.float32)  17.8 us
    dot_general x1, matrix products, shards(): jnp.dot(own, down_weight[0], preferred_element_type=jnp.float32)  16.6 us
    all_to_all x1, starting transfers between devices, shards(): lax.all_to_all(outgoing, 'sp', split_axis=0, concat_axis=0, tiled=True)  11.1 us
    all_to_all x1, starting transfers between devices, shards(): lax.all_to_all(expert_rows.reshape(received.shape), 'sp', split_axis=0, c...  10 us
    all_to_all x1, blocking collectives, shards(): lax.all_to_all(mixer_out, 'tp', split_axis=0, concat_axis=1, tiled=True)  4.53 us
  transfers between devices with their start and end apart: 6, of which 2 were waited for; matrix products, arithmetic and copies ran while one was open for 20% of the time, Pallas kernels for 0%

profile of v1, /device:TPU:1, one launch (start us, length us, event | category | flops | bytes accessed | tf_op | source)
XLA Modules:
  0.0 212.3 jit_solution(5489506482751713511)
XLA Ops:
  0.0 0.0 copy-start
  0.0 0.8 slice.57
  0.8 3.9 %collective-permute-start = (bf16[16,512]{1,0:T(8,128)(2,1)S(1)}, bf16[16,512]{1,0:T(8,128)(2,1)S(1)}, u32[]{:S(2)}, u32[]{:S(2)}) collective-permute-start(bf16[16,512]{1,0:T(8,128)(2,1)S(1)} %slice.57), channel_id=1, source_target_pairs={{0,2},{2,4},{4,6},{6,8},{8,10},{10,12},{12,14},{14,16},{16,18},{18... | collective-permute-start | bytes 49160 | tf_op jit(solution)/shard_map/ppermute | solution.py:10
  4.8 0.8 copy.39
  5.6 0.1 eq.57
  5.7 0.1 eq.53
  5.9 1.2 reduce-window.6
  7.1 0.2 slice_reduce_fusion
  7.4 0.1 fusion.31
  7.5 0.1 reduce_sum.39
  7.6 0.1 copy.42
  7.7 0.7 multiply_add_fusion
  8.4 0.4 fusion.4
  8.7 0.8 dynamic_slice.7
  9.5 0.0 collective-permute-done
  9.5 1.0 maximum_convert_fusion
  10.5 0.0 copy-start.2
  10.5 2.0 fusion.26
  12.5 0.0 copy-done
  12.5 0.3 convolution_bitcast_fusion
  12.8 0.0 copy-start.4
  12.8 0.3 reshape.171
  13.1 0.1 fusion.23
  13.3 4.5 %all_to_all.26 = bf16[2,128,512]{1,2,0:T(8,128)(2,1)S(1)} all-to-all(bf16[2,128,512]{1,2,0:T(8,128)(2,1)S(1)} %fusion.23), channel_id=1, replica_groups=mesh['sp'=64,'tp'=2] {'tp'}, dimensions={0} | all-to-all | bytes 524288 | tf_op jit(solution)/shard_map/all_to_all | solution.py:68
  17.8 0.0 copy-done.2
  17.8 3.0 %multiply_reduce_fusion = (f32[128]{0:T(128)S(1)}, f32[128,2048]{1,0:T(8,128)S(1)}) fusion(bf16[128,1024]{0,1:T(8,128)(2,1)S(1)} %bitcast.54, bf16[1024,2048]{1,0:T(8,128)(2,1)} %param.15, bf16[128,2048]{1,0:T(8,128)(2,1)S(1)} %copy-done.2), kind=kOutput, calls=%fused_computation.16 | convolution fusion | flops 538443648 | bytes 6029824 | tf_op jit(solution)/shard_map/dot_general | solution.py:69
  20.8 0.0 copy-done.4
  20.8 3.3 %convolution_convert_fusion = bf16[1024,2048]{1,0:T(8,128)(2,1)} fusion(pred[1024,128]{1,0:T(8,128)(4,1)S(1)} %fusion.4, f32[128,2048]{1,0:T(8,128)S(1)} %get-tuple-element.6, f32[2048]{0:T(1024)S(1)} %copy-done.4, f32[128]{0:T(128)S(1)} %add_rsqrt_fusion), kind=kOutput, calls=%fused_computation.3 | convolution fusion | flops 539754496 | bytes 5382656 | tf_op jit(solution)/shard_map/dot_general | solution.py:94
  24.1 11.1 %all-to-all-start.1 = ((bf16[64,16,2048]{2,1,0:T(8,128)(2,1)}), bf16[64,16,2048]{2,1,0:T(8,128)(2,1)}, u32[]{:S(2)}, u32[]{:S(2)}) async-start(bf16[64,16,2048]{2,1,0:T(8,128)(2,1)} %bitcast.52), calls=%async_computation.1 | async-start | bytes 8388608 | tf_op jit(solution)/shard_map/all_to_all | solution.py:98
  35.2 0.7 collective-permute-start.1
  35.9 0.1 collective-permute-start.2
  36.0 0.4 collective-permute-start.3
  36.4 52.2 %all-to-all-done.1 = bf16[64,16,2048]{2,1,0:T(8,128)(2,1)} async-done(((bf16[64,16,2048]{2,1,0:T(8,128)(2,1)}), bf16[64,16,2048]{2,1,0:T(8,128)(2,1)}, u32[]{:S(2)}, u32[]{:S(2)}) %all-to-all-start.1) | async-done | bytes 4194336 | tf_op jit(solution)/shard_map/all_to_all | solution.py:98
  88.6 9.9 %fusion.48 = f32[1024,1024]{1,0:T(8,128)} fusion(bf16[1024,2048]{1,0:T(8,128)(2,1)} %bitcast.5, bf16[1,2048,1024]{2,1,0:T(8,128)(2,1)} %param.20), kind=kOutput, calls=%fused_computation.107 | convolution fusion | flops 4294967296 | bytes 12582912 | tf_op jit(solution)/shard_map/dot_general | solution.py:15
  98.5 16.6 %fusion.5 = f32[1024,2048]{1,0:T(8,128)} fusion(f32[1024,1024]{1,0:T(8,128)} %fusion.48, bf16[1024,2048]{1,0:T(8,128)(2,1)} %bitcast.5, bf16[1,1024,2048]{2,1,0:T(8,128)(2,1)} %param.21, bf16[1,2048,1024]{2,1,0:T(8,128)(2,1)} %param.19), kind=kOutput, calls=%fused_computation.17 | convolution fusion | flops 8600420352 | bytes 25165824 | tf_op jit(solution)/shard_map/dot_general | solution.py:103
  115.2 0.0 collective-permute-done.1
  115.2 9.9 %fusion.58 = f32[1024,1024]{1,0:T(8,128)} fusion(bf16[1024,2048]{1,0:T(8,128)(2,1)} %bitcast.5, bf16[2048,1024]{1,0:T(8,128)(2,1)} %collective-permute-done.1), kind=kOutput, calls=%fused_computation.117 | convolution fusion | flops 4294967296 | bytes 12582912 | tf_op jit(solution)/shard_map/dot_general | solution.py:15
  125.1 0.0 collective-permute-done.2
  125.1 0.0 collective-permute-done.3
  125.1 17.8 %add_convert_fusion = bf16[1024,2048]{1,0:T(8,128)(2,1)} fusion(f32[1024,2048]{1,0:T(8,128)} %fusion.5, bf16[1024,2048]{1,0:T(8,128)(2,1)} %collective-permute-done.3, f32[1024,1024]{1,0:T(8,128)} %fusion.58, bf16[1024,2048]{1,0:T(8,128)(2,1)} %bitcast.5, bf16[2048,1024]{1,0:T(8,128)(2,1)} %collective-permute-done.2), kind=kOutput, calls=%fused_computation | convolution fusion | flops 8604614656 | bytes 29360128 | tf_op jit(solution)/shard_map/dot_general | solution.py:104
  142.9 0.0 copy-start.3
  142.9 10.0 %all-to-all-start.2 = ((bf16[64,16,2048]{2,1,0:T(8,128)(2,1)}), bf16[64,16,2048]{2,1,0:T(8,128)(2,1)}, u32[]{:S(2)}, u32[]{:S(2)}) async-start(bf16[64,16,2048]{2,1,0:T(8,128)(2,1)} %bitcast.53), calls=%async_computation.2 | async-start | bytes 8388608 | tf_op jit(solution)/shard_map/all_to_all | solution.py:106
  153.0 0.0 copy-done.3
  153.0 0.3 select_reduce_fusion
  153.4 52.1 %all-to-all-done.2 = bf16[64,16,2048]{2,1,0:T(8,128)(2,1)} async-done(((bf16[64,16,2048]{2,1,0:T(8,128)(2,1)}), bf16[64,16,2048]{2,1,0:T(8,128)(2,1)}, u32[]{:S(2)}, u32[]{:S(2)}) %all-to-all-start.2) | async-done | bytes 4194336 | tf_op jit(solution)/shard_map/all_to_all | solution.py:106
  205.4 0.0 copy-start.1
  205.4 3.0 %fusion.33 = f32[128,2048]{1,0:T(8,128)S(1)} fusion(bf16[1024,2048]{1,0:T(8,128)(2,1)} %bitcast.10, f32[128,1024]{1,0:T(8,128)S(1)} %select_reduce_fusion), kind=kOutput, calls=%fused_computation.66 | convolution fusion | flops 537001984 | bytes 5767168 | tf_op jit(solution)/shard_map/dot_general | solution.py:119
  208.4 3.9 %fusion.3 = bf16[128,2048]{1,0:T(8,128)(2,1)} fusion(f32[128,2048]{1,0:T(8,128)S(1)} %get-tuple-element.6, f32[128,2048]{1,0:T(8,128)S(1)} %fusion.33, bf16[1024,2048]{1,0:T(8,128)(2,1)} %bitcast.10, f32[128,1024]{1,0:T(8,128)S(1)} %select_reduce_fusion), kind=kOutput, calls=%fused_computation.9 | convolution fusion | flops 538181632 | bytes 7340032 | tf_op jit(solution)/shard_map/dot_general | solution.py:119
  212.3 0.0 copy-done.1
  (17 shorter events, 0.2 us)
Async XLA Ops:
  0.0 12.5 %copy-start = (bf16[4,256,256]{2,1,0:T(8,128)(2,1)S(1)}, bf16[4,256,256]{2,1,0:T(8,128)(2,1)}, u32[]{:S(2)}) copy-start(bf16[4,256,256]{2,1,0:T(8,128)(2,1)} %param.13) | copy-start | bytes 1572868
  0.8 8.7 %collective-permute-start = (bf16[16,512]{1,0:T(8,128)(2,1)S(1)}, bf16[16,512]{1,0:T(8,128)(2,1)S(1)}, u32[]{:S(2)}, u32[]{:S(2)}) collective-permute-start(bf16[16,512]{1,0:T(8,128)(2,1)S(1)} %slice.57), channel_id=1, source_target_pairs={{0,2},{2,4},{4,6},{6,8},{8,10},{10,12},{12,14},{14,16},{16,18},{18... | collective-permute-start | bytes 49160 | tf_op jit(solution)/shard_map/ppermute | solution.py:10
  10.5 7.3 %copy-start.2 = (bf16[128,2048]{1,0:T(8,128)(2,1)S(1)}, bf16[128,2048]{1,0:T(8,128)(2,1)}, u32[]{:S(2)}) copy-start(bf16[128,2048]{1,0:T(8,128)(2,1)} %param.12) | copy-start | bytes 1572868
  12.8 8.0 %copy-start.4 = (f32[2048]{0:T(1024)S(1)}, f32[2048]{0:T(1024)}, u32[]{:S(2)}) copy-start(f32[2048]{0:T(1024)} %param.16) | copy-start | bytes 24580
  24.1 64.5 %all-to-all-start.1 = ((bf16[64,16,2048]{2,1,0:T(8,128)(2,1)}), bf16[64,16,2048]{2,1,0:T(8,128)(2,1)}, u32[]{:S(2)}, u32[]{:S(2)}) async-start(bf16[64,16,2048]{2,1,0:T(8,128)(2,1)} %bitcast.52), calls=%async_computation.1 | async-start | bytes 8388608 | tf_op jit(solution)/shard_map/all_to_all | solution.py:98
  35.2 80.0 %collective-permute-start.1 = (bf16[2048,1024]{1,0:T(8,128)(2,1)}, bf16[2048,1024]{1,0:T(8,128)(2,1)}, u32[]{:S(2)}, u32[]{:S(2)}) collective-permute-start(bf16[2048,1024]{1,0:T(8,128)(2,1)} %bitcast.56), channel_id=1, source_target_pairs={{0,1},{1,0},{2,3},{3,2},{4,5},{5,4},{6,7},{7,6},{8,9},{9,8},{10,11... | collective-permute-start | bytes 12582920 | tf_op jit(solution)/shard_map/ppermute | solution.py:38
  35.9 89.2 %collective-permute-start.2 = (bf16[2048,1024]{1,0:T(8,128)(2,1)}, bf16[2048,1024]{1,0:T(8,128)(2,1)}, u32[]{:S(2)}, u32[]{:S(2)}) collective-permute-start(bf16[2048,1024]{1,0:T(8,128)(2,1)} %bitcast.57), channel_id=1, source_target_pairs={{0,1},{1,0},{2,3},{3,2},{4,5},{5,4},{6,7},{7,6},{8,9},{9,8},{10,11... | collective-permute-start | bytes 12582920 | tf_op jit(solution)/shard_map/ppermute | solution.py:37
  36.0 89.1 %collective-permute-start.3 = (bf16[1024,2048]{1,0:T(8,128)(2,1)}, bf16[1024,2048]{1,0:T(8,128)(2,1)}, u32[]{:S(2)}, u32[]{:S(2)}) collective-permute-start(bf16[1024,2048]{1,0:T(8,128)(2,1)} %bitcast.58), channel_id=1, source_target_pairs={{0,1},{1,0},{2,3},{3,2},{4,5},{5,4},{6,7},{7,6},{8,9},{9,8},{10,11... | collective-permute-start | bytes 12582920 | tf_op jit(solution)/shard_map/ppermute | solution.py:39
  142.9 10.0 %copy-start.3 = (f32[128,4]{0,1:T(4,128)S(1)}, f32[128,4]{0,1:T(4,128)}, u32[]{:S(2)}) copy-start(f32[128,4]{0,1:T(4,128)} %param.18) | copy-start | bytes 6148
  142.9 62.5 %all-to-all-start.2 = ((bf16[64,16,2048]{2,1,0:T(8,128)(2,1)}), bf16[64,16,2048]{2,1,0:T(8,128)(2,1)}, u32[]{:S(2)}, u32[]{:S(2)}) async-start(bf16[64,16,2048]{2,1,0:T(8,128)(2,1)} %bitcast.53), calls=%async_computation.2 | async-start | bytes 8388608 | tf_op jit(solution)/shard_map/all_to_all | solution.py:106
  205.4 6.8 %copy-start.1 = (bf16[4,256,256]{2,1,0:T(8,128)(2,1)S(1)}, bf16[4,256,256]{2,1,0:T(8,128)(2,1)}, u32[]{:S(2)}) copy-start(bf16[4,256,256]{2,1,0:T(8,128)(2,1)} %param.13) | copy-start | bytes 1572868

commit v2 on v1

v2 whole, which is shorter than its diff:
```python
import jax
import jax.numpy as jnp
from jax import lax
from jax.experimental import pallas as pl
from jax.experimental.pallas import tpu as pltpu
from jax.sharding import PartitionSpec as P

T = 256
R = 256
T2 = 256
HALO = 16
CAP = 16
PIECE = 256


def front_kernel(
    place_ref,
    halo_own,
    pool_input,
    halo_other,
    swapped,
    pool_weight,
    pool_gain,
    norm_gain,
    routes,
    out_weight_h,
    residual_h,
    outgoing_h,
    middle_ref,
    spot_ref,
    out_weight,
    residual,
    outgoing,
    s_weight,
    s_residual,
    s_out,
):
    rows = residual.shape[0]
    experts = spot_ref.shape[0]
    groups, group_dim, _ = pool_weight.shape
    weight_copy = pltpu.make_async_copy(out_weight_h, out_weight, s_weight)
    weight_copy.start()
    residual_copy = pltpu.make_async_copy(residual_h, residual, s_residual)
    residual_copy.start()
    core = place_ref[0]
    first = place_ref[1]
    lower = core == 0
    own = jnp.where(
        lower,
        jnp.concatenate([halo_own[...], pool_input[:rows, :]], axis=0).astype(jnp.float32),
        pool_input[rows - HALO :, :].astype(jnp.float32),
    )
    other = jnp.where(
        lower,
        jnp.concatenate([halo_other[...], swapped[:rows, :]], axis=0).astype(jnp.float32),
        swapped[...].astype(jnp.float32),
    )
    sides = (jnp.where(lower, own, other), jnp.where(lower, other, own))
    position = (first + 1 + lax.broadcasted_iota(jnp.int32, (rows, 1), 0)).astype(jnp.float32)
    mixed = []
    for group in range(groups):
        side = sides[group * 2 // groups]
        column = (group * group_dim) % side.shape[1]
        values = side[:, column : column + group_dim]
        total = values
        for step in range(group + 1):
            total = total + pltpu.roll(total, 1 << step, 0)
        window = float(2 << group)
        pooled = (total[HALO:] / jnp.minimum(position, window) - values[HALO:]).astype(jnp.bfloat16)
        grouped = jnp.dot(pooled, pool_weight[group], preferred_element_type=jnp.float32)
        span = slice(group * group_dim, (group + 1) * group_dim)
        mixed.append((grouped * pool_gain[:, span]).astype(jnp.bfloat16))
    expert_ids = lax.broadcasted_iota(jnp.int32, (experts, rows), 0)
    named = expert_ids == routes[0:1, :]
    for k in range(1, routes.shape[0]):
        named = jnp.logical_or(named, expert_ids == routes[k : k + 1, :])
    earlier = (
        lax.broadcasted_iota(jnp.int32, (rows, rows), 0)
        < lax.broadcasted_iota(jnp.int32, (rows, rows), 1)
    ).astype(jnp.float32).astype(jnp.bfloat16)
    ranks = jnp.dot(
        named.astype(jnp.float32).astype(jnp.bfloat16), earlier, preferred_element_type=jnp.float32
    )
    spot = jnp.where(named, ranks, -1.0)
    spot_ref[...] = spot
    picker = picked(spot).astype(jnp.bfloat16)
    weight_copy.wait()
    projected = jnp.dot(
        jnp.concatenate(mixed, axis=1), out_weight[...], preferred_element_type=jnp.float32
    )
    residual_copy.wait()
    middle = (residual[...].astype(jnp.float32) + projected).astype(jnp.bfloat16)
    middle_ref[...] = middle
    wide = middle.astype(jnp.float32)
    mean = jnp.mean(wide * wide, axis=1, keepdims=True)
    normed = (wide * lax.rsqrt(mean + 1e-05) * norm_gain[...]).astype(jnp.bfloat16)
    copies = []
    for piece in range(outgoing.shape[0] // PIECE):
        span = pl.ds(piece * PIECE, PIECE)
        outgoing[span, :] = jnp.dot(
            picker[piece * PIECE : (piece + 1) * PIECE], normed, preferred_element_type=jnp.float32
        ).astype(jnp.bfloat16)
        copy = pltpu.make_async_copy(outgoing.at[span], outgoing_h.at[span], s_out.at[piece])
        copy.start()
        copies.append(copy)
    for copy in copies:
        copy.wait()


def picked(spot):
    experts, rows = spot.shape
    slot = lax.broadcasted_iota(jnp.int32, (experts, CAP, rows), 1).astype(jnp.float32)
    chosen = jnp.broadcast_to(spot[:, None, :], (experts, CAP, rows)) == slot
    return jnp.where(chosen, 1.0, 0.0).reshape(experts * CAP, rows)


def front(place, halo_own, pool_input, halo_other, swapped, pool_weight, pool_gain, norm_gain, routes, out_weight, residual, experts):
    rows, width = residual.shape
    slots = experts * CAP
    vmem = pl.BlockSpec(memory_space=pltpu.VMEM)
    anywhere = pl.BlockSpec(memory_space=pl.ANY)
    return pl.pallas_call(
        front_kernel,
        out_shape=(
            jax.ShapeDtypeStruct((slots, width), jnp.bfloat16),
            jax.ShapeDtypeStruct((rows, width), jnp.bfloat16),
            jax.ShapeDtypeStruct((experts, rows), jnp.float32),
        ),
        in_specs=[pl.BlockSpec(memory_space=pltpu.SMEM)] + [vmem] * 8 + [anywhere] * 2,
        out_specs=(anywhere, vmem, vmem),
        scratch_shapes=[
            pltpu.VMEM(out_weight.shape, jnp.bfloat16),
            pltpu.VMEM((rows, width), jnp.bfloat16),
            pltpu.VMEM((slots, width), jnp.bfloat16),
            pltpu.SemaphoreType.DMA,
            pltpu.SemaphoreType.DMA,
            pltpu.SemaphoreType.DMA((slots // PIECE,)),
        ],
        cost_estimate=pl.CostEstimate(
            flops=4 * rows * width * slots, bytes_accessed=10 * slots * width // 2, transcendentals=0
        ),
        name="front",
    )(place, halo_own, pool_input, halo_other, swapped, pool_weight, pool_gain, norm_gain, routes, out_weight, residual)


def back_kernel(spot, routes, scores, middle, returned_h, out_ref, returned, sums, s_in):
    slots, width = returned.shape
    experts, rows = spot.shape
    pieces = slots // PIECE
    copies = []
    for piece in range(pieces):
        span = pl.ds(piece * PIECE, PIECE)
        copies.append(pltpu.make_async_copy(returned_h.at[span], returned.at[span], s_in.at[piece]))
        copies[-1].start()
    raised = jnp.exp(scores[...] - jnp.max(scores[...], axis=0, keepdims=True))
    weights = raised / jnp.sum(raised, axis=0, keepdims=True)
    expert_ids = lax.broadcasted_iota(jnp.int32, (experts, rows), 0)
    per_expert = jnp.zeros((experts, rows), jnp.float32)
    for k in range(routes.shape[0]):
        per_expert = per_expert + jnp.where(
            expert_ids == routes[k : k + 1, :], weights[k : k + 1, :], 0.0
        )
    spread = picked(spot[...]) * jnp.broadcast_to(
        per_expert[:, None, :], (experts, CAP, rows)
    ).reshape(slots, rows)
    spread = spread.T
    high = spread.astype(jnp.bfloat16)
    low = (spread - high.astype(jnp.float32)).astype(jnp.bfloat16)
    both = jnp.concatenate([high, low], axis=0)
    for piece in range(pieces):
        copies[piece].wait()
        part = jnp.dot(
            both[:, piece * PIECE : (piece + 1) * PIECE],
            returned[pl.ds(piece * PIECE, PIECE), :],
            preferred_element_type=jnp.float32,
        )
        part = part[:rows] + part[rows:]
        if piece == 0:
            sums[...] = part
        elif piece < pieces - 1:
            sums[...] += part
        else:
            out_ref[...] = (middle[...].astype(jnp.float32) + (sums[...] + part)).astype(jnp.bfloat16)


def back(spot, routes, scores, middle, returned):
    slots, width = returned.shape
    rows = middle.shape[0]
    vmem = pl.BlockSpec(memory_space=pltpu.VMEM)
    return pl.pallas_call(
        back_kernel,
        out_shape=jax.ShapeDtypeStruct((rows, width), jnp.bfloat16),
        in_specs=[vmem] * 4 + [pl.BlockSpec(memory_space=pl.ANY)],
        out_specs=vmem,
        scratch_shapes=[
            pltpu.VMEM((slots, width), jnp.bfloat16),
            pltpu.VMEM((rows, width), jnp.float32),
            pltpu.SemaphoreType.DMA((slots // PIECE,)),
        ],
        cost_estimate=pl.CostEstimate(
            flops=4 * rows * width * slots, bytes_accessed=2 * slots * width, transcendentals=0
        ),
        name="back",
    )(spot, routes, scores, middle, returned)


def activation(gate_pre, up_pre):
    clipped_gate = jnp.minimum(gate_pre, 7.0)
    clipped_up = jnp.clip(up_pre, -7.0, 7.0)
    return ((clipped_up + 1.0) * (clipped_gate * jax.nn.sigmoid(1.702 * clipped_gate))).astype(jnp.bfloat16)


def expert_kernel(rows_h, g0, u0, d0, g1, u1, d1, out_h, rows, act, wg, wu, wd, ob, sr, sg, su, sd, so):
    m, width = rows.shape
    half = g0.shape[1]
    n1 = half // T
    n2 = width // T2
    chunks = m // R
    def row_copy(c):
        return pltpu.make_async_copy(rows_h.at[pl.ds(c * R, R)], rows.at[pl.ds(c * R, R)], sr.at[c])
    def in_copies(gate, up, tile, slot):
        return (pltpu.make_async_copy(gate.at[:, pl.ds(tile * T, T)], wg.at[slot], sg.at[slot]),
                pltpu.make_async_copy(up.at[:, pl.ds(tile * T, T)], wu.at[slot], su.at[slot]))
    def down_copies(tile, slot):
        return (pltpu.make_async_copy(d0.at[:, pl.ds(tile * T2, T2)], wd.at[slot, pl.ds(0, half)], sd.at[slot, 0]),
                pltpu.make_async_copy(d1.at[:, pl.ds(tile * T2, T2)], wd.at[slot, pl.ds(half, half)], sd.at[slot, 1]))
    def fetch_in(step, slot):
        @pl.when(step < n1)
        def _():
            for c in in_copies(g0, u0, step, slot): c.start()
        @pl.when(jnp.logical_and(step >= n1, step < 2 * n1))
        def _():
            for c in in_copies(g1, u1, step - n1, slot): c.start()
    def fetch_down(step, slot):
        @pl.when(step < n2)
        def _():
            for c in down_copies(step, slot): c.start()
    first = in_copies(g0, u0, 0, 0)
    first[0].start(); row_copy(0).start(); first[1].start()
    for c in range(1, chunks): row_copy(c).start()
    fetch_in(1, 1)
    fetch_down(0, 0); fetch_down(1, 1)
    for c in range(chunks): row_copy(c).wait()
    @pl.loop(0, 2 * n1)
    def _(step):
        slot = step % 2
        for c in in_copies(g0, u0, 0, slot): c.wait()
        for c in range(chunks):
            part = rows[pl.ds(c * R, R), :]
            gate_pre = jnp.dot(part, wg[slot], preferred_element_type=jnp.float32)
            up_pre = jnp.dot(part, wu[slot], preferred_element_type=jnp.float32)
            act[step, pl.ds(c * R, R), :] = activation(gate_pre, up_pre)
        fetch_in(step + 2, slot)
    @pl.loop(0, n2)
    def _(step):
        slot = step % 2
        for c in down_copies(0, slot): c.wait()
        out_copy = pltpu.make_async_copy(ob.at[slot], out_h.at[:, pl.ds(step * T2, T2)], so.at[slot])
        @pl.when(step >= 2)
        def _(): out_copy.wait()
        for c in range(chunks):
            left = jnp.concatenate([act[s, pl.ds(c * R, R), :] for s in range(2 * n1)], axis=1)
            ob[slot, pl.ds(c * R, R), :] = jnp.dot(left, wd[slot], preferred_element_type=jnp.float32).astype(jnp.bfloat16)
        out_copy.start()
        fetch_down(step + 2, slot)
    for slot in range(2):
        pltpu.make_async_copy(ob.at[slot], out_h.at[:, pl.ds(0, T2)], so.at[slot]).wait()


def expert(rows, g0, u0, d0, g1, u1, d1):
    m, width = rows.shape
    half = g0.shape[1]
    anyspec = pl.BlockSpec(memory_space=pl.ANY)
    return pl.pallas_call(
        expert_kernel,
        out_shape=jax.ShapeDtypeStruct((m, width), jnp.bfloat16),
        in_specs=[anyspec] * 7,
        out_specs=anyspec,
        scratch_shapes=[
            pltpu.VMEM((m, width), jnp.bfloat16),
            pltpu.VMEM((2 * half // T, m, T), jnp.bfloat16),
            pltpu.VMEM((2, width, T), jnp.bfloat16),
            pltpu.VMEM((2, width, T), jnp.bfloat16),
            pltpu.VMEM((2, 2 * half, T2), jnp.bfloat16),
            pltpu.VMEM((2, m, T2), jnp.bfloat16),
            pltpu.SemaphoreType.DMA((m // R,)),
            pltpu.SemaphoreType.DMA((2,)),
            pltpu.SemaphoreType.DMA((2,)),
            pltpu.SemaphoreType.DMA((2, 2)),
            pltpu.SemaphoreType.DMA((2,)),
        ],
        cost_estimate=pl.CostEstimate(
            flops=12 * m * width * half,
            bytes_accessed=4 * m * width + 12 * width * half,
            transcendentals=2 * m * half,
        ),
        name="expert",
    )(rows, g0, u0, d0, g1, u1, d1)


def shards(
    pool_input,
    residual,
    pool_weight,
    pool_gain,
    out_weight,
    norm_gain,
    routes,
    route_scores,
    gate_weight,
    up_weight,
    down_weight,
):
    chips = lax.axis_size("sp")
    core = lax.axis_index("tp")
    rows, model_width = residual.shape
    experts = gate_weight.shape[0] * chips
    swap = [(0, 1), (1, 0)]
    both_axes = ("sp", "tp")
    tail_rows = pool_input[pool_input.shape[0] - HALO :]
    sent = lax.dynamic_slice_in_dim(pool_input, (1 - core) * (rows - HALO), rows + HALO, 0)
    halo_first = lax.ppermute(
        tail_rows, both_axes, [(2 * chip, 2 * chip + 2) for chip in range(chips - 1)]
    )
    halo_second = lax.ppermute(
        tail_rows, both_axes, [(2 * chip + 1, 2 * chip + 2) for chip in range(chips - 1)]
    )
    swapped = lax.ppermute(sent, "tp", swap)
    gate_own, up_own, down_own, halo_first, halo_second, swapped = lax.optimization_barrier(
        (gate_weight[0], up_weight[0], down_weight[0], halo_first, halo_second, swapped)
    )
    gate_other = lax.ppermute(gate_own, "tp", swap)
    up_other = lax.ppermute(up_own, "tp", swap)
    down_other = lax.ppermute(down_own, "tp", swap)
    place = jnp.stack([core, (lax.axis_index("sp") * 2 + core) * rows]).astype(jnp.int32)
    outgoing, middle, spot = front(
        place,
        halo_first,
        pool_input,
        halo_second,
        swapped,
        pool_weight,
        pool_gain[None, :],
        norm_gain[None, :],
        routes.T,
        out_weight,
        residual,
        experts,
    )
    received = lax.all_to_all(
        outgoing.reshape(experts, CAP, model_width), "sp", split_axis=0, concat_axis=0, tiled=True
    )
    expert_rows = expert(
        received.reshape(-1, model_width), gate_own, up_own, down_own, gate_other, up_other, down_other
    )
    returned = lax.all_to_all(
        expert_rows.reshape(received.shape), "sp", split_axis=0, concat_axis=0, tiled=True
    )
    return back(spot, routes.T, route_scores.T, middle, returned.reshape(-1, model_width))


def solution(mesh):
    return jax.shard_map(
        shards,
        mesh=mesh,
        in_specs=(
            P("sp", "tp"),
            P(("sp", "tp"), None),
            P(),
            P(),
            P(),
            P(),
            P(("sp", "tp"), None),
            P(("sp", "tp"), None),
            P("sp", None, "tp"),
            P("sp", None, "tp"),
            P("sp", "tp", None),
        ),
        out_specs=P(("sp", "tp"), None),
        check_vma=False,
    )
```

time: 214 us -> 179 us (0.84)
  blocking collectives: 4.53 us -> 121 us
  waiting for transfers between devices: 104 us -> 0.24 us
  matrix products: 67.7 us -> 0 us
  Pallas kernels: 0 us -> 45.3 us
  starting transfers between devices: 26.3 us -> 8.57 us
  other arithmetic: 6.01 us -> 0.61 us
    all_to_all x1 -> x2, blocking collectives: 4.53 us -> 121 us  [the longest x1 64 us: shards(): lax.all_to_all(outgoing.reshape(experts, CAP, model_width), 'sp', split_a...]
    all_to_all x2 -> x0, waiting for transfers between devices: 104 us -> none  [the longest x1 52.2 us: shards(): lax.all_to_all(outgoing, 'sp', split_axis=0, concat_axis=0, tiled=True)]
    dot_general x9 -> x0, matrix products: 67.7 us -> none  [the longest x2 19.9 us: hidden_half(): up_pre = jnp.dot(rows, up_half, preferred_element_type=jnp.float32)]
    pallas_call x0 -> x3, Pallas kernels: none -> 45.3 us  [the longest x1 33.1 us: expert(): pl.pallas_call(expert_kernel, out_shape=jax.ShapeDtypeStruct((m, width),...]
    all_to_all x2 -> x0, starting transfers between devices: 21.1 us -> none  [the longest x1 11.1 us: shards(): lax.all_to_all(outgoing, 'sp', split_axis=0, concat_axis=0, tiled=True)]
    ppermute x4 -> x6, starting transfers between devices: 5.16 us -> 8.57 us  [the longest x1 5.87 us: shards(): lax.ppermute(tail_rows, both_axes, [(2 * chip + 1, 2 * chip + 2) for chip...]
    convert_element_type x13 -> x0, other arithmetic: 3.22 us -> none  [the longest x1 2 us: shards(): (totals / counts - pool_input.astype(jnp.float32)).astype(jnp.bfloat16)]
  transfers between devices with their start and end apart: 6 -> 6, of which waited for: 2 -> 1; matrix products, arithmetic and copies ran while one was open for 20% -> 1% of each run, Pallas kernels for 0% -> 4%
where the time goes in v2:
time: 179 us; the launch traced here: 178 us
  blocking collectives  121 us (68%)
  Pallas kernels  45.3 us (25%)
  starting transfers between devices  8.57 us (5%)
    all_to_all x1, blocking collectives, shards(): lax.all_to_all(outgoing.reshape(experts, CAP, model_width), 'sp', split_a...  64 us
    all_to_all x1, blocking collectives, shards(): lax.all_to_all(expert_rows.reshape(received.shape), 'sp', split_axis=0, c...  57.2 us
    pallas_call x1, Pallas kernels, expert(): pl.pallas_call(expert_kernel, out_shape=jax.ShapeDtypeStruct((m, width),...  33.1 us
    pallas_call x1, Pallas kernels, front(): pl.pallas_call(front_kernel, out_shape=(jax.ShapeDtypeStruct((slots, widt...  7.66 us
    ppermute x1, starting transfers between devices, shards(): lax.ppermute(tail_rows, both_axes, [(2 * chip + 1, 2 * chip + 2) for chip...  5.87 us
    pallas_call x1, Pallas kernels, back(): pl.pallas_call(back_kernel, out_shape=jax.ShapeDtypeStruct((rows, width),...  4.56 us
  transfers between devices with their start and end apart: 6, of which 1 were waited for; matrix products, arithmetic and copies ran while one was open for 1% of the time, Pallas kernels for 4%

profile of v2, /device:TPU:1, one launch (start us, length us, event | category | flops | bytes accessed | tf_op | source)
XLA Modules:
  0.0 177.7 jit_solution(16579641851329138859)
XLA Ops:
  0.0 0.9 constant_dynamic-slice_fusion
  0.9 1.5 collective-permute-start.2
  2.4 0.7 slice.3
  3.1 0.7 collective-permute-start
  3.8 5.9 %collective-permute-start.1 = (bf16[16,512]{1,0:T(8,128)(2,1)S(1)}, bf16[16,512]{1,0:T(8,128)(2,1)S(1)}, u32[]{:S(2)}, u32[]{:S(2)}) collective-permute-start(bf16[16,512]{1,0:T(8,128)(2,1)S(1)} %slice.3), channel_id=1, source_target_pairs={{1,2},{3,4},{5,6},{7,8},{9,10},{11,12},{13,14},{15,16},{17,18},{19... | collective-permute-start | bytes 49160 | tf_op jit(solution)/shard_map/ppermute | solution.py:325
  9.6 0.6 pad_add_fusion.place_ref
  10.3 0.0 collective-permute-done.halo_own
  10.3 0.0 copy-start.1
  10.3 0.2 collective-permute-done.1.halo_other
  10.5 0.0 copy-start.2
  10.5 0.0 collective-permute-done.2.swapped
  10.5 0.0 copy-start
  10.5 0.0 collective-permute-start.3
  10.5 0.5 collective-permute-start.4
  11.0 0.1 collective-permute-start.5
  11.1 0.0 copy-done.1
  11.1 0.0 copy-done.2
  11.1 0.1 copy-done
  11.2 7.7 %front.1 = (bf16[1024,2048]{1,0:T(8,128)(2,1)}, bf16[128,2048]{1,0:T(8,128)(2,1)}, f32[64,128]{1,0:T(8,128)}) custom-call(s32[2]{0:T(128)} %pad_add_fusion.place_ref, bf16[16,512]{1,0:T(8,128)(2,1)} %copy-done.1, bf16[256,512]{1,0:T(8,128)(2,1)} %pool_input.1, bf16[16,512]{1,0:T(8,128)(2,1)} %copy-done.2, bf16[144,512]{1,0:T(8,128)(2,1)} %copy-done, ...), custom_call_target="tpu_custom_call" | custom-call | flops 1073741824 | bytes 10485760 | tf_op jit(solution)/shard_map/front/pallas_call | solution.py:122
  18.8 64.0 %all_to_all.10 = bf16[64,16,2048]{2,1,0:T(8,128)(2,1)} all-to-all(bf16[64,16,2048]{2,1,0:T(8,128)(2,1)} %bitcast.15), channel_id=1, replica_groups=mesh['sp'=64,'tp'=2] {'sp'}, dimensions={0} | all-to-all | bytes 8388608 | tf_op jit(solution)/shard_map/all_to_all | solution.py:350
  82.8 0.0 collective-permute-done.3.g1
  82.8 0.0 collective-permute-done.4.u1
  82.8 0.0 collective-permute-done.5.d1
  82.9 33.1 %expert.1 = bf16[1024,2048]{1,0:T(8,128)(2,1)} custom-call(bf16[1024,2048]{1,0:T(8,128)(2,1)} %bitcast.14, bf16[2048,1024]{1,0:T(8,128)(2,1)} %bitcast.23, bf16[2048,1024]{1,0:T(8,128)(2,1)} %bitcast.25, bf16[1024,2048]{1,0:T(8,128)(2,1)} %bitcast.27, bf16[2048,1024]{1,0:T(8,128)(2,1)} %collective-permute-done.3.g1, ...), custom_call_target="tpu_custom_call" | custom-call | flops 25769803776 | bytes 33554432 | tf_op jit(solution)/shard_map/expert/pallas_call | solution.py:274
  116.0 57.2 %all_to_all.11 = bf16[64,16,2048]{2,1,0:T(8,128)(2,1)} all-to-all(bf16[64,16,2048]{2,1,0:T(8,128)(2,1)} %bitcast.16), channel_id=1, replica_groups=mesh['sp'=64,'tp'=2] {'sp'}, dimensions={0} | all-to-all | bytes 8388608 | tf_op jit(solution)/shard_map/all_to_all | solution.py:356
  173.1 4.6 %back.1 = bf16[128,2048]{1,0:T(8,128)(2,1)} custom-call(f32[64,128]{1,0:T(8,128)} %get-tuple-element.17.spot, s32[4,128]{1,0:T(4,128)} %bitcast.19, f32[4,128]{1,0:T(4,128)} %bitcast.21, bf16[128,2048]{1,0:T(8,128)(2,1)} %get-tuple-element.18.middle, bf16[1024,2048]{1,0:T(8,128)(2,1)} %bitcast.13), custom_call_target="tpu_custom_call" | custom-call | flops 1073741824 | bytes 4194304 | tf_op jit(solution)/shard_map/back/pallas_call | solution.py:190
Async XLA Ops:
  0.9 9.6 %collective-permute-start.2 = (bf16[144,512]{1,0:T(8,128)(2,1)S(1)}, bf16[144,512]{1,0:T(8,128)(2,1)S(1)}, u32[]{:S(2)}, u32[]{:S(2)}) collective-permute-start(bf16[144,512]{1,0:T(8,128)(2,1)S(1)} %constant_dynamic-slice_fusion), channel_id=1, source_target_pairs={{0,1},{1,0},{2,3},{3,2},{4,5},{5,4},{6,7},{7,6},{8,9},{9,8},{10,11... | collective-permute-start | bytes 442376 | tf_op jit(solution)/shard_map/ppermute | solution.py:328
  3.1 7.2 %collective-permute-start = (bf16[16,512]{1,0:T(8,128)(2,1)S(1)}, bf16[16,512]{1,0:T(8,128)(2,1)S(1)}, u32[]{:S(2)}, u32[]{:S(2)}) collective-permute-start(bf16[16,512]{1,0:T(8,128)(2,1)S(1)} %slice.3), channel_id=1, source_target_pairs={{0,2},{2,4},{4,6},{6,8},{8,10},{10,12},{12,14},{14,16},{16,18},{18... | collective-permute-start | bytes 49160 | tf_op jit(solution)/shard_map/ppermute | solution.py:322
  3.8 6.7 %collective-permute-start.1 = (bf16[16,512]{1,0:T(8,128)(2,1)S(1)}, bf16[16,512]{1,0:T(8,128)(2,1)S(1)}, u32[]{:S(2)}, u32[]{:S(2)}) collective-permute-start(bf16[16,512]{1,0:T(8,128)(2,1)S(1)} %slice.3), channel_id=1, source_target_pairs={{1,2},{3,4},{5,6},{7,8},{9,10},{11,12},{13,14},{15,16},{17,18},{19... | collective-permute-start | bytes 49160 | tf_op jit(solution)/shard_map/ppermute | solution.py:325
  10.3 0.8 copy-start.1
  10.5 0.6 copy-start.2
  10.5 0.7 copy-start
  10.5 72.3 %collective-permute-start.3 = (bf16[2048,1024]{1,0:T(8,128)(2,1)}, bf16[2048,1024]{1,0:T(8,128)(2,1)}, u32[]{:S(2)}, u32[]{:S(2)}) collective-permute-start(bf16[2048,1024]{1,0:T(8,128)(2,1)} %bitcast.22), channel_id=1, source_target_pairs={{0,1},{1,0},{2,3},{3,2},{4,5},{5,4},{6,7},{7,6},{8,9},{9,8},{10,11... | collective-permute-start | bytes 12582920 | tf_op jit(solution)/shard_map/ppermute | solution.py:332
  10.5 72.3 %collective-permute-start.4 = (bf16[2048,1024]{1,0:T(8,128)(2,1)}, bf16[2048,1024]{1,0:T(8,128)(2,1)}, u32[]{:S(2)}, u32[]{:S(2)}) collective-permute-start(bf16[2048,1024]{1,0:T(8,128)(2,1)} %bitcast.24), channel_id=1, source_target_pairs={{0,1},{1,0},{2,3},{3,2},{4,5},{5,4},{6,7},{7,6},{8,9},{9,8},{10,11... | collective-permute-start | bytes 12582920 | tf_op jit(solution)/shard_map/ppermute | solution.py:333
  11.0 71.8 %collective-permute-start.5 = (bf16[1024,2048]{1,0:T(8,128)(2,1)}, bf16[1024,2048]{1,0:T(8,128)(2,1)}, u32[]{:S(2)}, u32[]{:S(2)}) collective-permute-start(bf16[1024,2048]{1,0:T(8,128)(2,1)} %bitcast.26), channel_id=1, source_target_pairs={{0,1},{1,0},{2,3},{3,2},{4,5},{5,4},{6,7},{7,6},{8,9},{9,8},{10,11... | collective-permute-start | bytes 12582920 | tf_op jit(solution)/shard_map/ppermute | solution.py:334
